TPU v7x, 32 devices: a whole 2x2x4 slice. The times are simulated.
32 devices in a mesh: grp: 2 (over y), fs: 4 (over z), tp: 4 (over x, core).
Axes of the slice: x: 2, y: 2, z: 4, core: 2. Of those that a mesh axis runs over, the one named last changes fastest.
Arguments:
- tokens: bfloat16 [512, 2048], P(('grp', 'fs')), parts along dimension 0, may hold values from -6 to 6
- routes: int32 [512, 2], P(('grp', 'fs')), parts along dimension 0, may hold values from 0 to 3, as said below
- route_logits: float32 [512, 2], P(('grp', 'fs')), parts along dimension 0, may hold values from -8 to 8
- gain: float32 [2048], P('fs'), may hold values from 0.1 to 1.9
- w_gate: float32 [4, 2048, 7168], P(None, 'fs', 'tp'), may hold values from -0.125 to 0.125
- w_up: float32 [4, 2048, 7168], P(None, 'fs', 'tp'), may hold values from -0.125 to 0.125
- w_down: float32 [4, 7168, 2048], P(None, 'fs', 'tp'), may hold values from -0.0625 to 0.0625
Outputs:
- gate_served: bfloat16 [8, 2048, 7168], P(('grp', 'tp'), None, 'fs'), parts along dimension 0
- up_served: bfloat16 [8, 2048, 7168], P(('grp', 'tp'), None, 'fs'), parts along dimension 0
- down_served: bfloat16 [8, 7168, 2048], P(('grp', 'tp'), 'fs'), parts along dimension 0
- mixed: bfloat16 [512, 2048], P(('grp', 'fs'), 'tp'), parts along dimension 0
There are 2 independent parts, one for each index of `grp`. A program takes and returns all parts, laid end to end along the dimension named above; an argument that names none is the same for every part. Nothing has to cross between parts.
Inputs may be any that keep to these rules, and one draw needn't show every extreme that they name: `routes`: each row names 2 different experts; every expert is named by some row.
All inputs are finite; a program needn't handle non-finite values.
Results may differ from a plain program's by a relative error of at most 0.0085.
Values may be sent and summed in bfloat16 or wider, within the bound.
A program may use at most 192 MiB of HBM per device.

v0:
```python
import jax
import jax.numpy as jnp
from jax import lax
from jax.sharding import PartitionSpec as P


def body(tokens, routes, route_logits, gain, w_gate, w_up, w_down):
    gate_cast = (w_gate * gain[None, :, None]).astype(jnp.bfloat16)
    up_cast = (w_up * gain[None, :, None]).astype(jnp.bfloat16)
    down_cast = w_down.astype(jnp.bfloat16)
    gate_tp, up_tp, down_served = (
        lax.all_to_all(gate_cast, "tp", split_axis=0, concat_axis=2, tiled=True),
        lax.all_to_all(up_cast, "tp", split_axis=0, concat_axis=2, tiled=True),
        lax.all_to_all(down_cast, "tp", split_axis=0, concat_axis=2, tiled=True),
    )
    gate_served, up_served = (
        lax.all_to_all(gate_tp, "fs", split_axis=2, concat_axis=1, tiled=True),
        lax.all_to_all(up_tp, "fs", split_axis=2, concat_axis=1, tiled=True),
    )
    values = tokens.astype(jnp.float32)
    mean_square = jnp.mean(values * values, axis=-1, keepdims=True)
    normed = (values * lax.rsqrt(mean_square + 1e-06)).astype(jnp.bfloat16)
    expert_id = lax.axis_index("tp")
    first = jax.nn.sigmoid(route_logits[:, 0] - route_logits[:, 1])
    second = jax.nn.sigmoid(route_logits[:, 1] - route_logits[:, 0])
    weight_col = first * (routes[:, 0] == expert_id).astype(jnp.float32)
    weight_col = (weight_col + second * (routes[:, 1] == expert_id).astype(jnp.float32)).astype(
        jnp.bfloat16
    )
    gate_local = gate_served[0]
    up_local = up_served[0]
    piece_rows = lax.all_gather(normed, "fs", axis=0, tiled=True)
    piece_weight = lax.all_gather(weight_col, "fs", axis=0, tiled=True)
    gate_act = jnp.dot(piece_rows, gate_local, preferred_element_type=jnp.float32)
    up_act = jnp.dot(piece_rows, up_local, preferred_element_type=jnp.float32)
    hidden_rows = jax.nn.silu(gate_act) * up_act * piece_weight[:, None].astype(jnp.float32)
    hidden = hidden_rows.astype(jnp.bfloat16)
    down_local = down_served[0]
    term = jnp.dot(hidden, down_local, preferred_element_type=jnp.float32)
    by_feature = lax.psum_scatter(term, "tp", scatter_dimension=1, tiled=True)
    mixed = lax.psum_scatter(by_feature, "fs", scatter_dimension=0, tiled=True)
    return (gate_served, up_served, down_served, mixed.astype(jnp.bfloat16))


def solution(mesh):
    return jax.shard_map(
        body,
        mesh=mesh,
        in_specs=(
            P(("grp", "fs"), None),
            P(("grp", "fs"), None),
            P(("grp", "fs"), None),
            P("fs"),
            P(None, "fs", "tp"),
            P(None, "fs", "tp"),
            P(None, "fs", "tp"),
        ),
        out_specs=(
            P(("grp", "tp"), None, "fs"),
            P(("grp", "tp"), None, "fs"),
            P(("grp", "tp"), "fs", None),
            P(("grp", "fs"), "tp"),
        ),
        check_vma=False,
    )
```

profile of v0, /device:TPU:0, one launch (start us, length us, event | category | flops | bytes accessed | tf_op | source)
XLA Modules:
  0.0 715.9 jit_solution(18152583940366378702)
XLA Ops:
  7.2 14.4 %copy.24 = f32[4,512,1792]{1,2,0:T(8,128)} copy(f32[4,512,1792]{2,1,0:T(8,128)} %param.11) | data formatting | bytes 29360128 | tf_op args[4]
  21.5 0.0 copy-start.1
  21.5 14.3 %copy.27 = f32[4,512,1792]{1,2,0:T(8,128)} copy(f32[4,512,1792]{2,1,0:T(8,128)} %param.12) | data formatting | bytes 29360128 | tf_op args[5]
  35.8 0.0 copy-done.1
  35.8 13.5 %multiply_convert_fusion = (bf16[4,512,1792]{1,2,0:T(8,128)(2,1)}, bf16[4,512,1792]{1,2,0:T(8,128)(2,1)S(1)}) fusion(f32[4,512,1792]{1,2,0:T(8,128)} %copy.27, f32[512]{0:T(512)S(1)} %copy-done.1, f32[4,512,1792]{1,2,0:T(8,128)} %copy.24), kind=kLoop, calls=%fused_computation | loop fusion | flops 14680064 | bytes 44042240 | tf_op jit(solution)/shard_map/convert_element_type | solution.py:9
  49.3 86.2 %all_to_all.90 = bf16[4,512,1792]{1,2,0:T(8,128)(2,1)} all-to-all(bf16[4,512,1792]{1,2,0:T(8,128)(2,1)S(1)} %get-tuple-element.17), channel_id=1, replica_groups=mesh['grp'=2,'fs'=4,'tp'=4] {'tp'}, dimensions={0} | all-to-all | bytes 14680064 | tf_op jit(solution)/shard_map/all_to_all | solution.py:12
  135.5 5.4 all-to-all-start.2
  140.9 13.7 %copy.39 = bf16[1,512,7168]{1,0,2:T(2,128)(2,1)} copy(bf16[1,512,7168]{1,2,0:T(8,128)(2,1)} %bitcast.47) | data formatting | bytes 14680064 | tf_op jit(solution)/shard_map/all_to_all | solution.py:12
  154.7 0.5 broadcast.43
  155.2 48.2 %reduce = bf16[7168,512]{1,0:T(8,128)(2,1)} reduce(bf16[7168,1,512]{2,1,0:T(2,128)(2,1)} %bitcast.43, bf16[]{:T(256)} %broadcast.43), dimensions={1}, to_apply=%bitcast.42.reduce_sub_computation | reduce | bytes 14680066
  203.4 9.0 %reshape.55 = bf16[4,2,458752]{2,1,0:T(2,128)(2,1)} reshape(bf16[7168,512]{1,0:T(8,128)(2,1)} %reduce) | data formatting | bytes 14680064
  212.4 10.5 %all-to-all-done.2 = bf16[4,512,1792]{1,2,0:T(8,128)(2,1)} async-done(((bf16[4,512,1792]{1,2,0:T(8,128)(2,1)}), bf16[4,512,1792]{1,2,0:T(8,128)(2,1)}, u32[]{:S(2)}, u32[]{:S(2)}) %all-to-all-start.2) | async-done | bytes 7340064 | tf_op jit(solution)/shard_map/all_to_all | solution.py:13
  222.8 5.7 all-to-all-start.1
  228.5 13.7 %copy.38 = bf16[1,512,7168]{1,0,2:T(2,128)(2,1)} copy(bf16[1,512,7168]{1,2,0:T(8,128)(2,1)} %bitcast.7) | data formatting | bytes 14680064 | tf_op jit(solution)/shard_map/all_to_all | solution.py:13
  242.2 48.2 %reduce.1 = bf16[7168,512]{1,0:T(8,128)(2,1)} reduce(bf16[7168,1,512]{2,1,0:T(2,128)(2,1)} %bitcast.44, bf16[]{:T(256)} %broadcast.43), dimensions={1}, to_apply=%bitcast.41.reduce_sub_computation | reduce | bytes 14680066
  290.4 9.0 %reshape.57 = bf16[4,2,458752]{2,1,0:T(2,128)(2,1)} reshape(bf16[7168,512]{1,0:T(8,128)(2,1)} %reduce.1) | data formatting | bytes 14680064
  299.4 90.4 %all-to-all-done.1 = bf16[4,2,458752]{2,1,0:T(2,128)(2,1)} async-done(((bf16[4,2,458752]{2,1,0:T(2,128)(2,1)}), bf16[4,2,458752]{2,1,0:T(2,128)(2,1)}, u32[]{:S(2)}, u32[]{:S(2)}) %all-to-all-start.1) | async-done | bytes 7340064 | tf_op jit(solution)/shard_map/all_to_all | solution.py:17
  389.8 5.5 all-to-all-start.3
  395.3 11.6 %copy.30 = bf16[4,1792,512]{1,2,0:T(8,128)(2,1)} copy(f32[4,1792,512]{2,1,0:T(8,128)} %param.13) | data formatting | bytes 22020096 | tf_op args[6]
  407.0 0.0 copy-start
  407.0 0.0 copy-start.5
  407.0 0.0 copy-start.2
  407.0 0.0 copy-start.3
  407.0 148.5 %all-to-all-done.3 = bf16[4,2,458752]{2,1,0:T(2,128)(2,1)} async-done(((bf16[4,2,458752]{2,1,0:T(2,128)(2,1)}), bf16[4,2,458752]{2,1,0:T(2,128)(2,1)}, u32[]{:S(2)}, u32[]{:S(2)}) %all-to-all-start.3) | async-done | bytes 7340064 | tf_op jit(solution)/shard_map/all_to_all | solution.py:18
  555.4 5.4 all-to-all-start.4
  560.9 0.0 all-gather.3.cloned.1.call-start
  560.9 0.0 copy-done
  560.9 0.2 fusion.3
  561.1 0.8 fusion.4
  561.9 0.0 all-gather.3.cloned.1.call-update
  561.9 0.0 reduce-scatter.3.cloned.1.call-start
  562.0 0.0 copy-done.5
  562.0 0.6 dynamic-slice
  563.2 0.0 copy-done.2
  563.3 0.0 copy-done.3
  563.3 0.2 dynamic-update-slice
  563.5 10.1 %all-reduce = bf16[256]{0:T(256)(128)(2,1)S(1)} all-reduce(bf16[256]{0:T(256)(128)(2,1)S(1)} %dynamic-update-slice), channel_id=2, replica_groups=mesh['grp'=2,'fs'=4,'tp'=4] {'fs'}, use_global_device_ids=true, to_apply=%add | all-reduce | flops 256 | bytes 1024
  573.7 11.3 %reshape.56 = bf16[7168,1,512]{2,1,0:T(2,128)(2,1)} reshape(bf16[4,2,458752]{2,1,0:T(2,128)(2,1)} %all-to-all-done.1) | data formatting | bytes 14680064
  585.0 10.4 %copy.34 = bf16[1,512,7168]{1,2,0:T(8,128)(2,1)} copy(bf16[1,512,7168]{1,0,2:T(2,128)(2,1)} %bitcast.45) | data formatting | bytes 14680064
  595.4 9.9 %copy.26 = bf16[1,4,512,1792]{3,2,1,0:T(8,128)(2,1)} copy(bf16[1,4,512,1792]{2,3,1,0:T(8,128)(2,1)} %bitcast.48) | data formatting | bytes 14680064 | tf_op jit(solution)/shard_map/all_to_all | solution.py:17
  605.3 11.3 %reshape.58 = bf16[7168,1,512]{2,1,0:T(2,128)(2,1)} reshape(bf16[4,2,458752]{2,1,0:T(2,128)(2,1)} %all-to-all-done.3) | data formatting | bytes 14680064
  616.6 10.4 %copy.35 = bf16[1,512,7168]{1,2,0:T(8,128)(2,1)} copy(bf16[1,512,7168]{1,0,2:T(2,128)(2,1)} %bitcast.46) | data formatting | bytes 14680064
  627.0 9.9 %copy.29 = bf16[1,4,512,1792]{3,2,1,0:T(8,128)(2,1)} copy(bf16[1,4,512,1792]{2,3,1,0:T(8,128)(2,1)} %bitcast.49) | data formatting | bytes 14680064 | tf_op jit(solution)/shard_map/all_to_all | solution.py:18
  637.0 0.0 all-gather.3.cloned.1.call-done
  637.0 0.0 copy-start.4
  637.0 5.5 fusion.7
  642.5 0.2 all-to-all-done.4
  642.8 0.0 copy-done.4
  642.8 11.1 %fusion.2 = f32[256,2048]{1,0:T(8,128)} fusion(bf16[1792,2048]{0,1:T(8,128)(2,1)} %bitcast.18, bf16[256,2048]{1,0:T(8,128)(2,1)S(1)} %copy-done.4, bf16[2048,1792]{1,0:T(8,128)(2,1)} %bitcast.52, f32[256,1792]{1,0:T(8,128)S(1)} %fusion.7, f32[256]{0:T(256)S(1)} %convert_element_type.41), kind=kOutput, calls=%fused_computation.5 | convolution fusion | flops 3761307648 | bytes 19661824 | tf_op jit(solution)/shard_map/dot_general | solution.py:39
  653.9 0.0 reduce-scatter.3.cloned.1.call-update
  653.9 0.0 reduce-scatter.5.cloned.1.call-start
  653.9 29.7 %reduce-scatter.3.cloned.1.call-done = f32[256,512]{1,0:T(8,128)} async-done(((f32[256,2048]{1,0:T(8,128)}), f32[256,512]{1,0:T(8,128)}) %reduce-scatter.3.cloned.1.call-update) | async-done | bytes 524304 | tf_op jit(solution)/shard_map/reduce_scatter | solution.py:40
  683.6 0.0 reduce-scatter.5.cloned.1.call-update
  683.7 10.4 %copy.33 = bf16[1,1792,2048]{2,1,0:T(8,128)(2,1)} copy(bf16[1,1792,2048]{1,2,0:T(8,128)(2,1)} %bitcast.12) | data formatting | bytes 14680064
  694.1 13.7 %reduce-scatter.5.cloned.1.call-done = f32[64,512]{1,0:T(8,128)} async-done(((f32[256,512]{1,0:T(8,128)}), f32[64,512]{1,0:T(8,128)}) %reduce-scatter.5.cloned.1.call-update) | async-done | bytes 131088 | tf_op jit(solution)/shard_map/reduce_scatter | solution.py:41
  707.8 1.5 convert_element_type.38
  (4 shorter events, 0.0 us)
Async XLA Ops:
  21.5 14.3 %copy-start.1 = (f32[512]{0:T(512)S(1)}, f32[512]{0:T(512)}, u32[]{:S(2)}) copy-start(f32[512]{0:T(512)} %param.10) | copy-start | bytes 6148
  135.5 87.3 %all-to-all-start.2 = ((bf16[4,512,1792]{1,2,0:T(8,128)(2,1)}), bf16[4,512,1792]{1,2,0:T(8,128)(2,1)}, u32[]{:S(2)}, u32[]{:S(2)}) async-start(bf16[4,512,1792]{1,2,0:T(8,128)(2,1)} %get-tuple-element.16), calls=%async_computation.2 | async-start | bytes 14680064 | tf_op jit(solution)/shard_map/all_to_all | solution.py:13
  222.8 167.0 %all-to-all-start.1 = ((bf16[4,2,458752]{2,1,0:T(2,128)(2,1)}), bf16[4,2,458752]{2,1,0:T(2,128)(2,1)}, u32[]{:S(2)}, u32[]{:S(2)}) async-start(bf16[4,2,458752]{2,1,0:T(2,128)(2,1)} %reshape.55), calls=%async_computation.1 | async-start | bytes 14680064 | tf_op jit(solution)/shard_map/all_to_all | solution.py:17
  389.8 165.6 %all-to-all-start.3 = ((bf16[4,2,458752]{2,1,0:T(2,128)(2,1)}), bf16[4,2,458752]{2,1,0:T(2,128)(2,1)}, u32[]{:S(2)}, u32[]{:S(2)}) async-start(bf16[4,2,458752]{2,1,0:T(2,128)(2,1)} %reshape.57), calls=%async_computation.3 | async-start | bytes 14680064 | tf_op jit(solution)/shard_map/all_to_all | solution.py:18
  407.0 154.0 %copy-start = (bf16[64,2048]{1,0:T(8,128)(2,1)S(1)}, bf16[64,2048]{1,0:T(8,128)(2,1)}, u32[]{:S(2)}) copy-start(bf16[64,2048]{1,0:T(8,128)(2,1)} %param.7) | copy-start | bytes 786436
  407.0 155.0 %copy-start.5 = (u32[32]{0:T(128)S(1)}, u32[32]{0:T(128)}, u32[]{:S(2)}) copy-start(u32[32]{0:T(128)} %constant.19) | copy-start | bytes 388
  407.0 156.3 %copy-start.2 = (s32[64,2]{0,1:T(2,128)S(1)}, s32[64,2]{0,1:T(2,128)}, u32[]{:S(2)}) copy-start(s32[64,2]{0,1:T(2,128)} %param.8) | copy-start | bytes 1540
  407.0 156.3 %copy-start.3 = (f32[64,2]{0,1:T(2,128)S(1)}, f32[64,2]{0,1:T(2,128)}, u32[]{:S(2)}) copy-start(f32[64,2]{0,1:T(2,128)} %param.9) | copy-start | bytes 1540
  555.4 87.3 %all-to-all-start.4 = ((bf16[4,1792,512]{1,2,0:T(8,128)(2,1)}), bf16[4,1792,512]{1,2,0:T(8,128)(2,1)}, u32[]{:S(2)}, u32[]{:S(2)}) async-start(bf16[4,1792,512]{1,2,0:T(8,128)(2,1)} %copy.30), calls=%async_computation.4 | async-start | bytes 14680064 | tf_op jit(solution)/shard_map/all_to_all | solution.py:14
  560.9 76.1 %all-gather.3.cloned.1.call-start = ((), (), s32[]{:S(2)}) async-start(), calls=%async_computation.7 | async-start | bytes 1310720 | tf_op jit(solution)/shard_map/all_gather | solution.py:32
  561.9 121.7 %reduce-scatter.3.cloned.1.call-start = ((), (), s32[]{:S(2)}) async-start(), calls=%async_computation.8 | async-start | bytes 2621440 | tf_op jit(solution)/shard_map/reduce_scatter | solution.py:40
  637.0 5.8 copy-start.4
  653.9 53.9 %reduce-scatter.5.cloned.1.call-start = ((), (), s32[]{:S(2)}) async-start(), calls=%async_computation.9 | async-start | bytes 655360 | tf_op jit(solution)/shard_map/reduce_scatter | solution.py:41
Sparse Core Ops, SparseCore 0:
  563.2 27.5 all-gather.2
  654.0 29.5 reduce-scatter.2
  685.9 21.8 reduce-scatter.4
where the time goes:
time: 718 us; the launch traced here: 716 us
  waiting for transfers between devices  293 us (41%)
  local copies, waits for them, and re-layouts  161 us (22%)
  other arithmetic  112 us (16%)
  blocking collectives  96.3 us (13%)
  starting transfers between devices  22.2 us (3%)
  matrix products  16.6 us (2%)
  between operations  14.5 us (2%)
    all_to_all x1, waiting for transfers between devices, body(): lax.all_to_all(up_tp, 'fs', split_axis=2, concat_axis=1, tiled=True)  148 us
    unnamed x26, local copies, waits for them, and re-layouts  113 us
    unnamed x3, other arithmetic  96.4 us
    all_to_all x1, waiting for transfers between devices, body(): lax.all_to_all(gate_tp, 'fs', split_axis=2, concat_axis=1, tiled=True)  90.4 us
    all_to_all x1, blocking collectives, body(): lax.all_to_all(gate_cast, 'tp', split_axis=0, concat_axis=2, tiled=True)  86.2 us
    reduce_scatter x1, waiting for transfers between devices, body(): by_feature = lax.psum_scatter(term, 'tp', scatter_dimension=1, tiled=True)  29.7 us
  transfers between devices with their start and end apart: 7, of which 6 were waited for; matrix products, arithmetic and copies ran while one was open for 33% of the time, Pallas kernels for 0%

commit v1 on v0

--- a/solution.py
+++ b/solution.py
@@ -2,6 +2,13 @@
 import jax.numpy as jnp
 from jax import lax
 from jax.sharding import PartitionSpec as P
+
+
+def stacked_exchange(block, axis, split, join):
+    devices = lax.axis_size(axis)
+    parts = jnp.stack(jnp.split(block, devices, axis=split), axis=0)
+    parts = lax.all_to_all(parts, axis, split_axis=0, concat_axis=0)
+    return jnp.concatenate(parts, axis=join)
 
 
 def body(tokens, routes, route_logits, gain, w_gate, w_up, w_down):
@@ -9,7 +16,7 @@
     up_cast = (w_up * gain[None, :, None]).astype(jnp.bfloat16)
     down_cast = w_down.astype(jnp.bfloat16)
     gate_tp, up_tp, down_served = (
-        lax.all_to_all(gate_cast, "tp", split_axis=0, concat_axis=2, tiled=True),
+        stacked_exchange(gate_cast, "tp", 0, 2),
         lax.all_to_all(up_cast, "tp", split_axis=0, concat_axis=2, tiled=True),
         lax.all_to_all(down_cast, "tp", split_axis=0, concat_axis=2, tiled=True),
     )

time: 718 us -> 719 us (level)
    all_to_all x1 -> x0, local copies, waits for them, and re-layouts: 13.7 us -> none  [body(): lax.all_to_all(gate_cast, 'tp', split_axis=0, concat_axis=2, tiled=True)]
    reshape x0 -> x1, local copies, waits for them, and re-layouts: none -> 13.7 us  [stacked_exchange(): return jnp.concatenate(parts, axis=join)]
where the time goes in v1:
time: 719 us; the launch traced here: 717 us
  waiting for transfers between devices  293 us (41%)
  local copies, waits for them, and re-layouts  161 us (22%)
  other arithmetic  113 us (16%)
  blocking collectives  96.3 us (13%)
  starting transfers between devices  22.2 us (3%)
  matrix products  16.6 us (2%)
  between operations  14.5 us (2%)
    all_to_all x1, waiting for transfers between devices, body(): lax.all_to_all(up_tp, 'fs', split_axis=2, concat_axis=1, tiled=True)  148 us
    unnamed x26, local copies, waits for them, and re-layouts  113 us
    unnamed x3, other arithmetic  96.4 us
    all_to_all x1, waiting for transfers between devices, body(): lax.all_to_all(gate_tp, 'fs', split_axis=2, concat_axis=1, tiled=True)  90.4 us
    all_to_all x1, blocking collectives, stacked_exchange(): parts = lax.all_to_all(parts, axis, split_axis=0, concat_axis=0)  86.2 us
    reduce_scatter x1, waiting for transfers between devices, body(): by_feature = lax.psum_scatter(term, 'tp', scatter_dimension=1, tiled=True)  29.7 us
  transfers between devices with their start and end apart: 7, of which 6 were waited for; matrix products, arithmetic and copies ran while one was open for 33% of the time, Pallas kernels for 0%

profile of v1, /device:TPU:0, one launch (start us, length us, event | category | flops | bytes accessed | tf_op | source)
XLA Modules:
  0.0 717.4 jit_solution(3461163147603590616)
XLA Ops:
  7.2 14.3 %copy.30 = f32[4,512,1792]{1,2,0:T(8,128)} copy(f32[4,512,1792]{2,1,0:T(8,128)} %param.11) | data formatting | bytes 29360128 | tf_op args[4]
  21.5 0.0 copy-start.1
  21.5 14.3 %copy.34 = f32[4,512,1792]{1,2,0:T(8,128)} copy(f32[4,512,1792]{2,1,0:T(8,128)} %param.12) | data formatting | bytes 29360128 | tf_op args[5]
  35.8 0.0 copy-done.1
  35.8 13.5 %multiply_convert_fusion = (bf16[4,512,1792]{1,2,0:T(8,128)(2,1)}, bf16[4,512,1792]{1,2,0:T(8,128)(2,1)S(1)}) fusion(f32[4,512,1792]{1,2,0:T(8,128)} %copy.34, f32[512]{0:T(512)S(1)} %copy-done.1, f32[4,512,1792]{1,2,0:T(8,128)} %copy.30), kind=kLoop, calls=%fused_computation | loop fusion | flops 14680064 | bytes 44042240 | tf_op jit(solution)/shard_map/convert_element_type | solution.py:16
  49.3 0.5 slice_bitcast_fusion.3
  49.8 1.0 pad_maximum_fusion
  50.8 86.2 %all_to_all.77 = bf16[4,1,512,1792]{2,3,1,0:T(8,128)(2,1)} all-to-all(bf16[4,1,512,1792]{2,3,1,0:T(8,128)(2,1)S(1)} %pad_maximum_fusion), channel_id=1, replica_groups=mesh['grp'=2,'fs'=4,'tp'=4] {'tp'}, dimensions={0} | all-to-all | bytes 14680064 | tf_op jit(solution)/shard_map/all_to_all | solution.py:10
  137.0 5.4 all-to-all-start.2
  142.4 13.7 %copy.46 = bf16[1,512,7168]{1,0,2:T(2,128)(2,1)} copy(bf16[1,512,7168]{1,2,0:T(8,128)(2,1)} %bitcast.55) | data formatting | bytes 14680064 | tf_op jit(solution)/shard_map/reshape | solution.py:11
  156.1 0.5 broadcast.43
  156.6 48.2 %reduce = bf16[7168,512]{1,0:T(8,128)(2,1)} reduce(bf16[7168,1,512]{2,1,0:T(2,128)(2,1)} %bitcast.51, bf16[]{:T(256)} %broadcast.43), dimensions={1}, to_apply=%bitcast.50.reduce_sub_computation | reduce | bytes 14680066
  204.9 9.0 %reshape.63 = bf16[4,2,458752]{2,1,0:T(2,128)(2,1)} reshape(bf16[7168,512]{1,0:T(8,128)(2,1)} %reduce) | data formatting | bytes 14680064
  213.8 10.5 %all-to-all-done.2 = bf16[4,512,1792]{1,2,0:T(8,128)(2,1)} async-done(((bf16[4,512,1792]{1,2,0:T(8,128)(2,1)}), bf16[4,512,1792]{1,2,0:T(8,128)(2,1)}, u32[]{:S(2)}, u32[]{:S(2)}) %all-to-all-start.2) | async-done | bytes 7340064 | tf_op jit(solution)/shard_map/all_to_all | solution.py:20
  224.3 5.7 all-to-all-start.1
  230.0 13.7 %copy.45 = bf16[1,512,7168]{1,0,2:T(2,128)(2,1)} copy(bf16[1,512,7168]{1,2,0:T(8,128)(2,1)} %bitcast.11) | data formatting | bytes 14680064 | tf_op jit(solution)/shard_map/all_to_all | solution.py:20
  243.7 48.2 %reduce.1 = bf16[7168,512]{1,0:T(8,128)(2,1)} reduce(bf16[7168,1,512]{2,1,0:T(2,128)(2,1)} %bitcast.52, bf16[]{:T(256)} %broadcast.43), dimensions={1}, to_apply=%bitcast.49.reduce_sub_computation | reduce | bytes 14680066
  291.9 9.0 %reshape.65 = bf16[4,2,458752]{2,1,0:T(2,128)(2,1)} reshape(bf16[7168,512]{1,0:T(8,128)(2,1)} %reduce.1) | data formatting | bytes 14680064
  300.9 90.4 %all-to-all-done.1 = bf16[4,2,458752]{2,1,0:T(2,128)(2,1)} async-done(((bf16[4,2,458752]{2,1,0:T(2,128)(2,1)}), bf16[4,2,458752]{2,1,0:T(2,128)(2,1)}, u32[]{:S(2)}, u32[]{:S(2)}) %all-to-all-start.1) | async-done | bytes 7340064 | tf_op jit(solution)/shard_map/all_to_all | solution.py:24
  391.3 5.5 all-to-all-start.3
  396.8 11.6 %copy.37 = bf16[4,1792,512]{1,2,0:T(8,128)(2,1)} copy(f32[4,1792,512]{2,1,0:T(8,128)} %param.13) | data formatting | bytes 22020096 | tf_op args[6]
  408.5 0.0 copy-start
  408.5 0.0 copy-start.5
  408.5 0.0 copy-start.2
  408.5 0.0 copy-start.3
  408.5 148.5 %all-to-all-done.3 = bf16[4,2,458752]{2,1,0:T(2,128)(2,1)} async-done(((bf16[4,2,458752]{2,1,0:T(2,128)(2,1)}), bf16[4,2,458752]{2,1,0:T(2,128)(2,1)}, u32[]{:S(2)}, u32[]{:S(2)}) %all-to-all-start.3) | async-done | bytes 7340064 | tf_op jit(solution)/shard_map/all_to_all | solution.py:25
  556.9 5.4 all-to-all-start.4
  562.4 0.0 all-gather.3.cloned.1.call-start
  562.4 0.0 copy-done
  562.4 0.2 fusion.3
  562.6 0.8 fusion.4
  563.4 0.0 all-gather.3.cloned.1.call-update
  563.4 0.0 reduce-scatter.3.cloned.1.call-start
  563.5 0.0 copy-done.5
  563.5 0.6 dynamic-slice
  564.8 0.0 copy-done.2
  564.8 0.0 copy-done.3
  564.8 0.2 dynamic-update-slice
  565.0 10.1 %all-reduce = bf16[256]{0:T(256)(128)(2,1)S(1)} all-reduce(bf16[256]{0:T(256)(128)(2,1)S(1)} %dynamic-update-slice), channel_id=2, replica_groups=mesh['grp'=2,'fs'=4,'tp'=4] {'fs'}, use_global_device_ids=true, to_apply=%add | all-reduce | flops 256 | bytes 1024
  575.2 11.3 %reshape.64 = bf16[7168,1,512]{2,1,0:T(2,128)(2,1)} reshape(bf16[4,2,458752]{2,1,0:T(2,128)(2,1)} %all-to-all-done.1) | data formatting | bytes 14680064
  586.5 10.4 %copy.41 = bf16[1,512,7168]{1,2,0:T(8,128)(2,1)} copy(bf16[1,512,7168]{1,0,2:T(2,128)(2,1)} %bitcast.53) | data formatting | bytes 14680064
  596.9 9.9 %copy.33 = bf16[1,4,512,1792]{3,2,1,0:T(8,128)(2,1)} copy(bf16[1,4,512,1792]{2,3,1,0:T(8,128)(2,1)} %bitcast.56) | data formatting | bytes 14680064 | tf_op jit(solution)/shard_map/all_to_all | solution.py:24
  606.8 11.3 %reshape.66 = bf16[7168,1,512]{2,1,0:T(2,128)(2,1)} reshape(bf16[4,2,458752]{2,1,0:T(2,128)(2,1)} %all-to-all-done.3) | data formatting | bytes 14680064
  618.1 10.4 %copy.42 = bf16[1,512,7168]{1,2,0:T(8,128)(2,1)} copy(bf16[1,512,7168]{1,0,2:T(2,128)(2,1)} %bitcast.54) | data formatting | bytes 14680064
  628.5 9.9 %copy.36 = bf16[1,4,512,1792]{3,2,1,0:T(8,128)(2,1)} copy(bf16[1,4,512,1792]{2,3,1,0:T(8,128)(2,1)} %bitcast.57) | data formatting | bytes 14680064 | tf_op jit(solution)/shard_map/all_to_all | solution.py:25
  638.5 0.0 all-gather.3.cloned.1.call-done
  638.5 0.0 copy-start.4
  638.5 5.5 fusion.7
  644.0 0.3 all-to-all-done.4
  644.3 0.0 copy-done.4
  644.3 11.1 %fusion.2 = f32[256,2048]{1,0:T(8,128)} fusion(bf16[1792,2048]{0,1:T(8,128)(2,1)} %bitcast.22, bf16[256,2048]{1,0:T(8,128)(2,1)S(1)} %copy-done.4, bf16[2048,1792]{1,0:T(8,128)(2,1)} %bitcast.60, f32[256,1792]{1,0:T(8,128)S(1)} %fusion.7, f32[256]{0:T(256)S(1)} %convert_element_type.41), kind=kOutput, calls=%fused_computation.10 | convolution fusion | flops 3761307648 | bytes 19661824 | tf_op jit(solution)/shard_map/dot_general | solution.py:46
  655.4 0.0 reduce-scatter.3.cloned.1.call-update
  655.4 0.0 reduce-scatter.5.cloned.1.call-start
  655.5 29.7 %reduce-scatter.3.cloned.1.call-done = f32[256,512]{1,0:T(8,128)} async-done(((f32[256,2048]{1,0:T(8,128)}), f32[256,512]{1,0:T(8,128)}) %reduce-scatter.3.cloned.1.call-update) | async-done | bytes 524304 | tf_op jit(solution)/shard_map/reduce_scatter | solution.py:47
  685.1 0.0 reduce-scatter.5.cloned.1.call-update
  685.2 10.4 %copy.40 = bf16[1,1792,2048]{2,1,0:T(8,128)(2,1)} copy(bf16[1,1792,2048]{1,2,0:T(8,128)(2,1)} %bitcast.16) | data formatting | bytes 14680064
  695.6 13.7 %reduce-scatter.5.cloned.1.call-done = f32[64,512]{1,0:T(8,128)} async-done(((f32[256,512]{1,0:T(8,128)}), f32[64,512]{1,0:T(8,128)}) %reduce-scatter.5.cloned.1.call-update) | async-done | bytes 131088 | tf_op jit(solution)/shard_map/reduce_scatter | solution.py:48
  709.3 1.5 convert_element_type.38
  (4 shorter events, 0.0 us)
Async XLA Ops:
  21.5 14.3 %copy-start.1 = (f32[512]{0:T(512)S(1)}, f32[512]{0:T(512)}, u32[]{:S(2)}) copy-start(f32[512]{0:T(512)} %param.10) | copy-start | bytes 6148
  137.0 87.3 %all-to-all-start.2 = ((bf16[4,512,1792]{1,2,0:T(8,128)(2,1)}), bf16[4,512,1792]{1,2,0:T(8,128)(2,1)}, u32[]{:S(2)}, u32[]{:S(2)}) async-start(bf16[4,512,1792]{1,2,0:T(8,128)(2,1)} %get-tuple-element.20), calls=%async_computation.2 | async-start | bytes 14680064 | tf_op jit(solution)/shard_map/all_to_all | solution.py:20
  224.3 167.0 %all-to-all-start.1 = ((bf16[4,2,458752]{2,1,0:T(2,128)(2,1)}), bf16[4,2,458752]{2,1,0:T(2,128)(2,1)}, u32[]{:S(2)}, u32[]{:S(2)}) async-start(bf16[4,2,458752]{2,1,0:T(2,128)(2,1)} %reshape.63), calls=%async_computation.1 | async-start | bytes 14680064 | tf_op jit(solution)/shard_map/all_to_all | solution.py:24
  391.3 165.6 %all-to-all-start.3 = ((bf16[4,2,458752]{2,1,0:T(2,128)(2,1)}), bf16[4,2,458752]{2,1,0:T(2,128)(2,1)}, u32[]{:S(2)}, u32[]{:S(2)}) async-start(bf16[4,2,458752]{2,1,0:T(2,128)(2,1)} %reshape.65), calls=%async_computation.3 | async-start | bytes 14680064 | tf_op jit(solution)/shard_map/all_to_all | solution.py:25
  408.5 154.0 %copy-start = (bf16[64,2048]{1,0:T(8,128)(2,1)S(1)}, bf16[64,2048]{1,0:T(8,128)(2,1)}, u32[]{:S(2)}) copy-start(bf16[64,2048]{1,0:T(8,128)(2,1)} %param.7) | copy-start | bytes 786436
  408.5 155.0 %copy-start.5 = (u32[32]{0:T(128)S(1)}, u32[32]{0:T(128)}, u32[]{:S(2)}) copy-start(u32[32]{0:T(128)} %constant.19) | copy-start | bytes 388
  408.5 156.3 %copy-start.2 = (s32[64,2]{0,1:T(2,128)S(1)}, s32[64,2]{0,1:T(2,128)}, u32[]{:S(2)}) copy-start(s32[64,2]{0,1:T(2,128)} %param.8) | copy-start | bytes 1540
  408.5 156.3 %copy-start.3 = (f32[64,2]{0,1:T(2,128)S(1)}, f32[64,2]{0,1:T(2,128)}, u32[]{:S(2)}) copy-start(f32[64,2]{0,1:T(2,128)} %param.9) | copy-start | bytes 1540
  556.9 87.3 %all-to-all-start.4 = ((bf16[4,1792,512]{1,2,0:T(8,128)(2,1)}), bf16[4,1792,512]{1,2,0:T(8,128)(2,1)}, u32[]{:S(2)}, u32[]{:S(2)}) async-start(bf16[4,1792,512]{1,2,0:T(8,128)(2,1)} %copy.37), calls=%async_computation.4 | async-start | bytes 14680064 | tf_op jit(solution)/shard_map/all_to_all | solution.py:21
  562.4 76.1 %all-gather.3.cloned.1.call-start = ((), (), s32[]{:S(2)}) async-start(), calls=%async_computation.7 | async-start | bytes 1310720 | tf_op jit(solution)/shard_map/all_gather | solution.py:39
  563.4 121.7 %reduce-scatter.3.cloned.1.call-start = ((), (), s32[]{:S(2)}) async-start(), calls=%async_computation.8 | async-start | bytes 2621440 | tf_op jit(solution)/shard_map/reduce_scatter | solution.py:47
  638.5 5.8 copy-start.4
  655.4 53.9 %reduce-scatter.5.cloned.1.call-start = ((), (), s32[]{:S(2)}) async-start(), calls=%async_computation.9 | async-start | bytes 655360 | tf_op jit(solution)/shard_map/reduce_scatter | solution.py:48
Sparse Core Ops, SparseCore 0:
  564.7 27.5 all-gather.2
  655.5 29.5 reduce-scatter.2
  687.4 21.8 reduce-scatter.4
